TPU v7x, 32 devices: a whole 2x2x4 slice. The times are simulated.
32 devices in a mesh: kv: 8 (over z, y), tp: 4 (over x, core).
Axes of the slice: x: 2, y: 2, z: 4, core: 2. Of those that a mesh axis runs over, the one named last changes fastest.
Arguments:
- tokens: bfloat16 [4096, 2048], P('kv'), may hold values from -18 to 18
- w_query: bfloat16 [2048, 1024], P(None, 'tp'), may hold values from -0.125 to 0.125
- w_key: bfloat16 [2048, 256], P(None, 'tp'), may hold values from -0.125 to 0.125
- w_value: bfloat16 [2048, 256], P(None, 'tp'), may hold values from -18 to 18
- w_out: bfloat16 [1024, 2048], P(None, 'tp'), may hold values from -0.1875 to 0.1875
- out_gain: float32 [1024], replicated, may hold values from 0.1 to 1.9
- chosen: int32 [4, 64, 8], P('tp', 'kv'), may hold values from -1 to 63, as said below
Outputs:
- mixed_out: bfloat16 [4096, 2048], P('kv', 'tp')
Inputs may be any that keep to these rules, and one draw needn't show every extreme that they name: chosen[h, b, 0] is b itself; the other entries of a row are distinct key blocks lying wholly before block b, or -1, placed after all named blocks; for each key head h, the query blocks on one index of kv (its 512 positions) name, together, at most one key block of head h held by any other index of kv.
All inputs are finite; a program needn't handle non-finite values.
Results may differ from a plain program's by a relative error of at most 0.024.
Values may be sent and summed in bfloat16 or wider, within the bound.
No kernel may reach another device: no remote copies, remote signals or barrier semaphores. Data moves between devices by JAX's collectives and lax.ppermute only.
A program may use at most 64 MiB of HBM per device.

v0:
```python
import jax
import jax.numpy as jnp
from jax import lax
from jax.sharding import PartitionSpec as P

HQ = 16
HD = 64
BLK = 64
SEL = 8
rope_base = 500000.0
norm_eps = 1e-06


def rotate(vectors, positions):
    half_size = vectors.shape[-1] // 2
    frequency = rope_base ** (-jnp.arange(half_size, dtype=jnp.float32) / half_size)
    angles = positions.astype(jnp.float32)[:, None] * frequency[None, :]
    cosine = jnp.cos(angles)[:, None, :]
    sine_wave = jnp.sin(angles)[:, None, :]
    lower_half = vectors[..., :half_size]
    upper_half = vectors[..., half_size:]
    return jnp.concatenate(
        [
            lower_half * cosine - upper_half * sine_wave,
            upper_half * cosine + lower_half * sine_wave,
        ],
        axis=-1,
    )


def per_device(tokens, w_query, w_key, w_value, w_out, out_gain, chosen):
    count_kv = lax.axis_size("kv")
    kv_place = lax.axis_index("kv")
    row_count = tokens.shape[0]
    block_count = row_count // BLK
    feat_width = w_query.shape[1]
    head_count = feat_width // HD
    positions = kv_place * row_count + jnp.arange(row_count, dtype=jnp.int32)
    queries = rotate(
        jnp.dot(tokens, w_query, preferred_element_type=jnp.float32).reshape(
            row_count, head_count, HD
        ),
        positions,
    ).astype(jnp.bfloat16)
    key_rows = (
        rotate(
            jnp.dot(tokens, w_key, preferred_element_type=jnp.float32).reshape(row_count, 1, HD),
            positions,
        )
        .astype(jnp.bfloat16)
        .reshape(row_count, HD)
    )
    value_rows = jnp.dot(tokens, w_value, preferred_element_type=jnp.float32).astype(jnp.bfloat16)
    local_pairs = jnp.concatenate([key_rows, value_rows], axis=1).reshape(block_count, BLK, 2 * HD)
    chosen_ids = chosen[0]
    usable = chosen_ids >= 0
    owners = jnp.where(usable, chosen_ids // block_count, kv_place)
    local_index = jnp.where(usable, chosen_ids % block_count, 0)
    remote = usable & (owners != kv_place)
    peer_ids = jnp.arange(count_kv, dtype=jnp.int32)
    matches = remote[:, :, None] & (owners[:, :, None] == peer_ids[None, None, :])
    wanted = jnp.max(jnp.where(matches, local_index[:, :, None], -1), axis=(0, 1))
    asked_for = lax.all_to_all(
        wanted.reshape(count_kv, 1), "kv", split_axis=0, concat_axis=0, tiled=True
    )[:, 0]
    outgoing = jnp.where(
        (asked_for >= 0)[:, None, None],
        local_pairs[jnp.maximum(asked_for, 0)],
        jnp.zeros((), jnp.bfloat16),
    )
    arrived = lax.all_to_all(outgoing, "kv", split_axis=0, concat_axis=0, tiled=True)
    pool_pairs = jnp.concatenate([arrived, local_pairs], axis=0)
    slot_index = jnp.where(owners == kv_place, count_kv + local_index, owners)
    selected = pool_pairs[slot_index]
    pair_count = block_count // 2
    offsets = jnp.arange(BLK, dtype=jnp.int32)
    score_scale = HD ** (-0.5)

    def attend(bundle):
        query_part, stacked, pair_ids, pair_usable, query_pos = bundle
        key_part = stacked[..., :HD]
        value_part = stacked[..., HD:]
        scores = (
            jnp.einsum("pqhd,pskd->phqsk", query_part, key_part, preferred_element_type=jnp.float32)
            * score_scale
        )
        key_pos = pair_ids[:, :, None] * BLK + offsets
        allowed = pair_usable[:, None, :, None] & (
            key_pos[:, None, :, :] <= query_pos[:, :, None, None]
        )
        scores = jnp.where(allowed[:, None], scores, -jnp.inf)
        peak_score = jnp.max(scores, axis=(3, 4), keepdims=True)
        weights = jnp.exp(scores - peak_score)
        softmax_w = (weights / jnp.sum(weights, axis=(3, 4), keepdims=True)).astype(jnp.bfloat16)
        mixed_out = jnp.einsum(
            "phqsk,pskd->pqhd", softmax_w, value_part, preferred_element_type=jnp.float32
        )
        return mixed_out.astype(jnp.bfloat16)

    attended = lax.map(
        attend,
        (
            queries.reshape(pair_count, 2, BLK, head_count, HD),
            selected.reshape(pair_count, 2, SEL, BLK, 2 * HD),
            chosen_ids.reshape(pair_count, 2, SEL),
            usable.reshape(pair_count, 2, SEL),
            positions.reshape(pair_count, 2, BLK),
        ),
    ).reshape(row_count, feat_width)
    attn_f32 = attended.astype(jnp.float32)
    squares = lax.psum(jnp.sum(attn_f32 * attn_f32, axis=1), "tp")
    gain_part = lax.dynamic_slice_in_dim(out_gain, lax.axis_index("tp") * feat_width, feat_width)
    scaled = (attn_f32 * gain_part[None, :]).astype(jnp.bfloat16)
    product = jnp.dot(
        lax.all_gather(scaled, "tp", axis=1, tiled=True), w_out, preferred_element_type=jnp.float32
    )
    inverse = lax.rsqrt(squares / (HQ * HD) + norm_eps)
    return (inverse[:, None] * product).astype(jnp.bfloat16)


def solution(mesh):
    return jax.shard_map(
        per_device,
        mesh=mesh,
        in_specs=(
            P("kv", None),
            P(None, "tp"),
            P(None, "tp"),
            P(None, "tp"),
            P(None, "tp"),
            P(),
            P("tp", "kv", None),
        ),
        out_specs=P("kv", "tp"),
        check_vma=False,
    )
```

profile of v0, /device:TPU:0, one launch (start us, length us, event | category | flops | bytes accessed | tf_op | source)
XLA Modules:
  0.0 87.1 jit_solution(12271367534152278380)
XLA Ops:
  6.5 0.8 fusion.20
  7.4 0.7 compare_and_fusion.1
  8.2 0.7 copy.36
  8.9 7.3 %all-to-all-start = ((s32[8,1,1]{2,1,0:T(1,128)}), s32[8,1,1]{2,1,0:T(1,128)S(1)}, u32[]{:S(2)}, u32[]{:S(2)}) async-start(s32[8,1,1]{2,1,0:T(1,128)} %copy.36), calls=%async_computation | async-start | bytes 8192 | tf_op jit(solution)/shard_map/all_to_all | solution.py:63
  16.2 0.7 compare_select_fusion
  16.9 1.7 %convolution_bitcast_fusion.1 = f32[512,1,64]{0,2,1:T(8,128)S(1)} fusion(bf16[512,2048]{1,0:T(8,128)(2,1)S(1)} %copy-done, bf16[2048,64]{0,1:T(8,128)(2,1)} %param.11), kind=kOutput, calls=%fused_computation.26 | convolution fusion | flops 134217728 | bytes 2490368 | tf_op jit(solution)/shard_map/dot_general | solution.py:47
  19.6 0.8 convolution_convert_fusion
  20.4 2.0 %fusion.34 = f32[512,256]{0,1:T(8,128)S(1)} fusion(bf16[512,2048]{1,0:T(8,128)(2,1)S(1)} %copy-done, bf16[2048,256]{1,0:T(8,128)(2,1)} %param.10), kind=kOutput, calls=%fused_computation.93 | convolution fusion | flops 536870912 | bytes 3670016 | tf_op jit(solution)/shard_map/dot_general | solution.py:40
  22.9 1.6 %pad_maximum_fusion = bf16[4,2,64,4,64]{2,1,0,4,3:T(2,128)(2,1)} fusion(bf16[4,2,64,4,32]{2,1,0,4,3:T(2,128)(2,1)S(1)} %concatenate.35, bf16[4,2,64,4,32]{2,1,0,4,3:T(2,128)(2,1)S(1)} %concatenate.34), kind=kLoop, calls=%fused_computation.29 | loop fusion | flops 131072 | bytes 524288 | tf_op jit(solution)/shard_map/concatenate | solution.py:22
  25.9 0.7 broadcast_select_fusion
  26.6 6.0 %all-to-all-start.1 = ((bf16[8,64,128]{2,1,0:T(8,128)(2,1)}), bf16[8,64,128]{2,1,0:T(8,128)(2,1)S(1)}, u32[]{:S(2)}, u32[]{:S(2)}) async-start(bf16[8,64,128]{2,1,0:T(8,128)(2,1)} %broadcast_select_fusion), calls=%async_computation.1 | async-start | bytes 262144 | tf_op jit(solution)/shard_map/all_to_all | solution.py:71
  32.7 0.8 dynamic_slice.23
  33.4 6.5 %all-to-all-done.1 = bf16[8,64,128]{2,1,0:T(8,128)(2,1)S(1)} async-done(((bf16[8,64,128]{2,1,0:T(8,128)(2,1)}), bf16[8,64,128]{2,1,0:T(8,128)(2,1)S(1)}, u32[]{:S(2)}, u32[]{:S(2)}) %all-to-all-start.1) | async-done | bytes 131104 | tf_op jit(solution)/shard_map/all_to_all | solution.py:71
  40.1 0.7 gather_fusion.1
  40.8 17.1 %while.11 = (s32[]{:T(128)}, bf16[4,2,64,4,64]{2,4,3,1,0:T(8,128)(2,1)}, bf16[4,2,8,64,128]{4,3,2,1,0:T(8,128)(2,1)S(1)}, pred[4,2,8]{2,1,0:T(4,128)(4,1)S(1)}, ...) while((s32[]{:T(128)}, ...), condition=%wide.region_4.5_spmd.clone, body=%wide.region_1.4_spmd.clone.sunk | while | flops 69369872 | bytes 13193617 | solution.py:100
  41.8 1.0 %constant_dynamic-slice_fusion.4 = bf16[1,2,64,4,64]{2,1,0,4,3:T(2,128)(2,1)S(1)} fusion(bf16[4,2,64,4,64]{2,1,0,4,3:T(2,128)(2,1)} %get-tuple-element.185, s32[]{:T(128)} %get-tuple-element.171), kind=kLoop, calls=%fused_computation.18.clone.1 | loop fusion | bytes 131076 | tf_op jit(solution)/shard_map/while/body/jit(dynamic_index_in_dim)/dynamic_slice | solution.py:100
  43.9 1.2 %fusion.52 = bf16[4,2,64,4,64]{2,4,3,1,0:T(8,128)(2,1)} fusion(bf16[4,2,64,4,64]{2,4,3,1,0:T(8,128)(2,1)} %get-tuple-element.172, s32[]{:T(128)} %get-tuple-element.171, f32[2,4,64,8,64]{2,4,1,3,0:T(8,128)S(1)} %get-tuple-element.161, f32[2,4,64]{2,1,0:T(4,128)S(1)} %fusion.51, f32[2,4,64]{2,1,0:T(4,128)S(1)} %get-tuple-element.162, ...), kind=kOutput, calls=%fused_computation.10.clone.1 | convolution fusion | flops 34373632 | bytes 1446400 | tf_op jit(solution)/shard_map/while/body/eval_jaxpr/phqsk,pskd->pqhd/dot_general | solution.py:95
  46.1 1.0 %constant_dynamic-slice_fusion.4 = bf16[1,2,64,4,64]{2,1,0,4,3:T(2,128)(2,1)S(1)} fusion(bf16[4,2,64,4,64]{2,1,0,4,3:T(2,128)(2,1)} %get-tuple-element.185, s32[]{:T(128)} %get-tuple-element.171), kind=kLoop, calls=%fused_computation.18.clone.1 | loop fusion | bytes 131076 | tf_op jit(solution)/shard_map/while/body/jit(dynamic_index_in_dim)/dynamic_slice | solution.py:100
  48.1 1.2 %fusion.52 = bf16[4,2,64,4,64]{2,4,3,1,0:T(8,128)(2,1)} fusion(bf16[4,2,64,4,64]{2,4,3,1,0:T(8,128)(2,1)} %get-tuple-element.172, s32[]{:T(128)} %get-tuple-element.171, f32[2,4,64,8,64]{2,4,1,3,0:T(8,128)S(1)} %get-tuple-element.161, f32[2,4,64]{2,1,0:T(4,128)S(1)} %fusion.51, f32[2,4,64]{2,1,0:T(4,128)S(1)} %get-tuple-element.162, ...), kind=kOutput, calls=%fused_computation.10.clone.1 | convolution fusion | flops 34373632 | bytes 1446400 | tf_op jit(solution)/shard_map/while/body/eval_jaxpr/phqsk,pskd->pqhd/dot_general | solution.py:95
  49.7 0.6 copy-done.1
  50.4 1.0 %constant_dynamic-slice_fusion.4 = bf16[1,2,64,4,64]{2,1,0,4,3:T(2,128)(2,1)S(1)} fusion(bf16[4,2,64,4,64]{2,1,0,4,3:T(2,128)(2,1)} %get-tuple-element.185, s32[]{:T(128)} %get-tuple-element.171), kind=kLoop, calls=%fused_computation.18.clone.1 | loop fusion | bytes 131076 | tf_op jit(solution)/shard_map/while/body/jit(dynamic_index_in_dim)/dynamic_slice | solution.py:100
  52.4 1.2 %fusion.52 = bf16[4,2,64,4,64]{2,4,3,1,0:T(8,128)(2,1)} fusion(bf16[4,2,64,4,64]{2,4,3,1,0:T(8,128)(2,1)} %get-tuple-element.172, s32[]{:T(128)} %get-tuple-element.171, f32[2,4,64,8,64]{2,4,1,3,0:T(8,128)S(1)} %get-tuple-element.161, f32[2,4,64]{2,1,0:T(4,128)S(1)} %fusion.51, f32[2,4,64]{2,1,0:T(4,128)S(1)} %get-tuple-element.162, ...), kind=kOutput, calls=%fused_computation.10.clone.1 | convolution fusion | flops 34373632 | bytes 1446400 | tf_op jit(solution)/shard_map/while/body/eval_jaxpr/phqsk,pskd->pqhd/dot_general | solution.py:95
  54.0 0.6 copy-done.1
  54.7 1.0 %constant_dynamic-slice_fusion.4 = bf16[1,2,64,4,64]{2,1,0,4,3:T(2,128)(2,1)S(1)} fusion(bf16[4,2,64,4,64]{2,1,0,4,3:T(2,128)(2,1)} %get-tuple-element.185, s32[]{:T(128)} %get-tuple-element.171), kind=kLoop, calls=%fused_computation.18.clone.1 | loop fusion | bytes 131076 | tf_op jit(solution)/shard_map/while/body/jit(dynamic_index_in_dim)/dynamic_slice | solution.py:100
  56.7 1.2 %fusion.52 = bf16[4,2,64,4,64]{2,4,3,1,0:T(8,128)(2,1)} fusion(bf16[4,2,64,4,64]{2,4,3,1,0:T(8,128)(2,1)} %get-tuple-element.172, s32[]{:T(128)} %get-tuple-element.171, f32[2,4,64,8,64]{2,4,1,3,0:T(8,128)S(1)} %get-tuple-element.161, f32[2,4,64]{2,1,0:T(4,128)S(1)} %fusion.51, f32[2,4,64]{2,1,0:T(4,128)S(1)} %get-tuple-element.162, ...), kind=kOutput, calls=%fused_computation.10.clone.1 | convolution fusion | flops 34373632 | bytes 1446400 | tf_op jit(solution)/shard_map/while/body/eval_jaxpr/phqsk,pskd->pqhd/dot_general | solution.py:95
  57.9 1.3 %copy.41 = f32[4,2,64,4,64]{4,3,2,1,0:T(4,128)S(1)} copy(bf16[4,2,64,4,64]{2,4,3,1,0:T(8,128)(2,1)} %get-tuple-element.47) | data formatting | bytes 786432 | tf_op jit(solution)/shard_map/convert_element_type | solution.py:110
  59.3 1.4 %reshape.350 = f32[512,256]{1,0:T(8,128)} reshape(f32[4,2,64,4,64]{4,3,2,1,0:T(4,128)S(1)} %copy.41) | data formatting | bytes 1048576 | tf_op jit(solution)/shard_map/convert_element_type | solution.py:110
  60.7 1.8 %multiply_convert_fusion = bf16[512,256]{1,0:T(8,128)(2,1)} fusion(f32[512,256]{1,0:T(8,128)} %reshape.350, f32[256]{0:T(256)S(1)} %dynamic_slice.23), kind=kLoop, calls=%fused_computation.30 | loop fusion | flops 262144 | bytes 787456 | tf_op jit(solution)/shard_map/convert_element_type | solution.py:113
  62.5 1.2 %multiply_reduce_fusion = f32[4,2,64]{2,1,0:T(2,128)S(1)} fusion(bf16[4,2,64,4,64]{2,4,3,1,0:T(8,128)(2,1)} %get-tuple-element.47), kind=kLoop, calls=%fused_computation.28 | loop fusion | flops 392704 | bytes 264192 | tf_op jit(solution)/shard_map/reduce_sum | solution.py:111
  63.8 5.6 %psum.7 = f32[512]{0:T(512)S(1)} all-reduce(f32[512]{0:T(512)S(1)} %reduce_sum.21), channel_id=1, replica_groups=mesh['kv'=8,'tp'=4] {'tp'}, use_global_device_ids=true, to_apply=%region_6.7 | all-reduce | flops 512 | bytes 4096 | tf_op jit(solution)/shard_map/psum | solution.py:111
  69.4 7.8 %all-gather.2.cloned.1.call-done = bf16[512,1024]{1,0:T(8,128)(2,1)} async-done(((bf16[512,256]{1,0:T(8,128)(2,1)}), bf16[512,1024]{1,0:T(8,128)(2,1)}) %all-gather.2.cloned.1.call-update) | async-done | bytes 1048592 | tf_op jit(solution)/shard_map/all_gather | solution.py:115
  77.3 3.0 %fusion.10 = bf16[512,512]{1,0:T(8,128)(2,1)} fusion(bf16[512,1024]{1,0:T(8,128)(2,1)} %all-gather.2.cloned.1.call-done, bf16[1024,512]{1,0:T(8,128)(2,1)} %param.13, f32[512]{0:T(512)S(1)} %add_rsqrt_fusion), kind=kOutput, calls=%fused_computation.25 | convolution fusion | flops 537395200 | bytes 2623488 | tf_op jit(solution)/shard_map/dot_general | solution.py:114
  (83 shorter events, 9.9 us)
Async XLA Ops:
  6.5 10.4 %copy-start = (bf16[512,2048]{1,0:T(8,128)(2,1)S(1)}, bf16[512,2048]{1,0:T(8,128)(2,1)}, u32[]{:S(2)}) copy-start(bf16[512,2048]{1,0:T(8,128)(2,1)} %param.9) | copy-start | bytes 6291460
  6.5 13.0 %copy-start.3 = (bf16[2048,64]{0,1:T(8,128)(2,1)S(1)}, bf16[2048,64]{0,1:T(8,128)(2,1)}, u32[]{:S(2)}) copy-start(bf16[2048,64]{0,1:T(8,128)(2,1)} %param.12) | copy-start | bytes 786436
  8.9 15.9 %all-to-all-start = ((s32[8,1,1]{2,1,0:T(1,128)}), s32[8,1,1]{2,1,0:T(1,128)S(1)}, u32[]{:S(2)}, u32[]{:S(2)}) async-start(s32[8,1,1]{2,1,0:T(1,128)} %copy.36), calls=%async_computation | async-start | bytes 8192 | tf_op jit(solution)/shard_map/all_to_all | solution.py:63
  22.4 11.0 %copy-start.4 = (s32[1,8,8]{2,1,0:T(8,128)S(1)}, s32[1,8,8]{2,1,0:T(8,128)}, u32[]{:S(2)}) copy-start(s32[1,8,8]{2,1,0:T(8,128)} %param.15) | copy-start | bytes 772
  26.6 13.3 %all-to-all-start.1 = ((bf16[8,64,128]{2,1,0:T(8,128)(2,1)}), bf16[8,64,128]{2,1,0:T(8,128)(2,1)S(1)}, u32[]{:S(2)}, u32[]{:S(2)}) async-start(bf16[8,64,128]{2,1,0:T(8,128)(2,1)} %broadcast_select_fusion), calls=%async_computation.1 | async-start | bytes 262144 | tf_op jit(solution)/shard_map/all_to_all | solution.py:71
  32.6 44.7 %all-gather.2.cloned.1.call-start = ((), (), s32[]{:S(2)}) async-start(), calls=%async_computation.2 | async-start | bytes 1310720 | tf_op jit(solution)/shard_map/all_gather | solution.py:115
  40.8 1.0 %copy-start.1 = (bf16[4,2,8,64,128]{4,3,2,1,0:T(8,128)(2,1)}, bf16[4,2,8,64,128]{4,3,2,1,0:T(8,128)(2,1)S(1)}, u32[]{:S(2)}) copy-start(bf16[4,2,8,64,128]{4,3,2,1,0:T(8,128)(2,1)S(1)} %get-tuple-element.181) | copy-start | bytes 3145732 | tf_op jit(solution)/shard_map/while
  43.9 1.2 %copy-start.2 = (bf16[4,2,8,64,128]{4,3,2,1,0:T(8,128)(2,1)S(1)}, bf16[4,2,8,64,128]{4,3,2,1,0:T(8,128)(2,1)}, u32[]{:S(2)}) copy-start(bf16[4,2,8,64,128]{4,3,2,1,0:T(8,128)(2,1)} %copy-done.1) | copy-start | bytes 3145732 | tf_op jit(solution)/shard_map/while
  45.1 1.0 %copy-start.1 = (bf16[4,2,8,64,128]{4,3,2,1,0:T(8,128)(2,1)}, bf16[4,2,8,64,128]{4,3,2,1,0:T(8,128)(2,1)S(1)}, u32[]{:S(2)}) copy-start(bf16[4,2,8,64,128]{4,3,2,1,0:T(8,128)(2,1)S(1)} %get-tuple-element.181) | copy-start | bytes 3145732 | tf_op jit(solution)/shard_map/while
  48.1 1.2 %copy-start.2 = (bf16[4,2,8,64,128]{4,3,2,1,0:T(8,128)(2,1)S(1)}, bf16[4,2,8,64,128]{4,3,2,1,0:T(8,128)(2,1)}, u32[]{:S(2)}) copy-start(bf16[4,2,8,64,128]{4,3,2,1,0:T(8,128)(2,1)} %copy-done.1) | copy-start | bytes 3145732 | tf_op jit(solution)/shard_map/while
  49.4 1.0 %copy-start.1 = (bf16[4,2,8,64,128]{4,3,2,1,0:T(8,128)(2,1)}, bf16[4,2,8,64,128]{4,3,2,1,0:T(8,128)(2,1)S(1)}, u32[]{:S(2)}) copy-start(bf16[4,2,8,64,128]{4,3,2,1,0:T(8,128)(2,1)S(1)} %get-tuple-element.181) | copy-start | bytes 3145732 | tf_op jit(solution)/shard_map/while
  52.4 1.2 %copy-start.2 = (bf16[4,2,8,64,128]{4,3,2,1,0:T(8,128)(2,1)S(1)}, bf16[4,2,8,64,128]{4,3,2,1,0:T(8,128)(2,1)}, u32[]{:S(2)}) copy-start(bf16[4,2,8,64,128]{4,3,2,1,0:T(8,128)(2,1)} %copy-done.1) | copy-start | bytes 3145732 | tf_op jit(solution)/shard_map/while
  53.7 1.0 %copy-start.1 = (bf16[4,2,8,64,128]{4,3,2,1,0:T(8,128)(2,1)}, bf16[4,2,8,64,128]{4,3,2,1,0:T(8,128)(2,1)S(1)}, u32[]{:S(2)}) copy-start(bf16[4,2,8,64,128]{4,3,2,1,0:T(8,128)(2,1)S(1)} %get-tuple-element.181) | copy-start | bytes 3145732 | tf_op jit(solution)/shard_map/while
  56.7 1.2 %copy-start.2 = (bf16[4,2,8,64,128]{4,3,2,1,0:T(8,128)(2,1)S(1)}, bf16[4,2,8,64,128]{4,3,2,1,0:T(8,128)(2,1)}, u32[]{:S(2)}) copy-start(bf16[4,2,8,64,128]{4,3,2,1,0:T(8,128)(2,1)} %copy-done.1) | copy-start | bytes 3145732 | tf_op jit(solution)/shard_map/while
Sparse Core Ops, SparseCore 0:
  62.6 14.5 all-gather.1
where the time goes:
time: 87.9 us; the launch traced here: 87.1 us
  matrix products  14.5 us (16%)
  waiting for transfers between devices  14.3 us (16%)
  local copies, waits for them, and re-layouts  13.6 us (15%)
  between operations  13.6 us (15%)
  starting transfers between devices  13.3 us (15%)
  other arithmetic  11.9 us (14%)
  blocking collectives  5.63 us (6%)
    all_gather x1, waiting for transfers between devices, per_device(): lax.all_gather(scaled, 'tp', axis=1, tiled=True)  7.83 us
    all_to_all x1, starting transfers between devices, per_device(): lax.all_to_all(wanted.reshape(count_kv, 1), 'kv', split_axis=0, concat_ax...  7.31 us
    all_to_all x1, waiting for transfers between devices, per_device(): lax.all_to_all(outgoing, 'kv', split_axis=0, concat_axis=0, tiled=True)  6.5 us
    all_to_all x1, starting transfers between devices, per_device(): lax.all_to_all(outgoing, 'kv', split_axis=0, concat_axis=0, tiled=True)  6 us
    psum x1, blocking collectives, per_device(): squares = lax.psum(jnp.sum(attn_f32 * attn_f32, axis=1), 'tp')  5.63 us
    dot_general x4, matrix products, attend(): jnp.einsum('phqsk,pskd->pqhd', softmax_w, value_part, preferred_element_t...  4.94 us
    dynamic_slice x8, local copies, waits for them, and re-layouts, per_device(): lax.map(attend, (queries.reshape(pair_count, 2, BLK, head_count, HD), sel...  4.53 us
    dot_general x1, matrix products, per_device(): jnp.dot(lax.all_gather(scaled, 'tp', axis=1, tiled=True), w_out, preferre...  3.04 us
  transfers between devices with their start and end apart: 3, of which 2 were waited for; matrix products, arithmetic and copies ran while one was open for 12% of the time, Pallas kernels for 0%

commit v1 on v0

--- a/solution.py
+++ b/solution.py
@@ -9,6 +9,13 @@
 SEL = 8
 rope_base = 500000.0
 norm_eps = 1e-06
+
+
+def swapped_in(x, mesh_axis, dim):
+    size = lax.axis_size(mesh_axis)
+    pieces = jnp.stack([x for _ in range(size)])
+    pieces = lax.all_to_all(pieces, mesh_axis, split_axis=0, concat_axis=0)
+    return jnp.concatenate(pieces, axis=dim)
 
 
 def rotate(vectors, positions):
@@ -111,9 +118,7 @@
     squares = lax.psum(jnp.sum(attn_f32 * attn_f32, axis=1), "tp")
     gain_part = lax.dynamic_slice_in_dim(out_gain, lax.axis_index("tp") * feat_width, feat_width)
     scaled = (attn_f32 * gain_part[None, :]).astype(jnp.bfloat16)
-    product = jnp.dot(
-        lax.all_gather(scaled, "tp", axis=1, tiled=True), w_out, preferred_element_type=jnp.float32
-    )
+    product = jnp.dot(swapped_in(scaled, "tp", 1), w_out, preferred_element_type=jnp.float32)
     inverse = lax.rsqrt(squares / (HQ * HD) + norm_eps)
     return (inverse[:, None] * product).astype(jnp.bfloat16)
 

time: 87.9 us -> 79.4 us (0.903)
  between operations: 13.6 us -> 0.18 us
  blocking collectives: 5.63 us -> 14.6 us
  waiting for transfers between devices: 14.3 us -> 6.55 us
  starting transfers between devices: 13.3 us -> 16.8 us
  local copies, waits for them, and re-layouts: 13.6 us -> 14.8 us
    psum x1, blocking collectives: 5.63 us -> 14.6 us  [per_device(): squares = lax.psum(jnp.sum(attn_f32 * attn_f32, axis=1), 'tp')]
    all_gather x1 -> x0, waiting for transfers between devices: 7.83 us -> none  [per_device(): lax.all_gather(scaled, 'tp', axis=1, tiled=True)]
    all_to_all x0 -> x1, starting transfers between devices: none -> 3.51 us  [swapped_in(): pieces = lax.all_to_all(pieces, mesh_axis, split_axis=0, concat_axis=0)]
    another operation x0 -> x1, local copies, waits for them, and re-layouts: none -> 1.07 us  [swapped_in(): pieces = jnp.stack([x for _ in range(size)])]
  transfers between devices with their start and end apart: 3 -> 3, of which waited for: 2 -> 1; matrix products, arithmetic and copies ran while one was open for 12% -> 13% of each run, Pallas kernels for 0% -> 0%
where the time goes in v1:
time: 79.4 us; the launch traced here: 78.6 us
  starting transfers between devices  16.8 us (21%)
  local copies, waits for them, and re-layouts  14.8 us (19%)
  blocking collectives  14.6 us (18%)
  matrix products  14.3 us (18%)
  other arithmetic  11.2 us (14%)
  waiting for transfers between devices  6.55 us (8%)
    psum x1, blocking collectives, per_device(): squares = lax.psum(jnp.sum(attn_f32 * attn_f32, axis=1), 'tp')  14.6 us
    all_to_all x1, starting transfers between devices, per_device(): lax.all_to_all(wanted.reshape(count_kv, 1), 'kv', split_axis=0, concat_ax...  7.31 us
    all_to_all x1, waiting for transfers between devices, per_device(): lax.all_to_all(outgoing, 'kv', split_axis=0, concat_axis=0, tiled=True)  6.55 us
    all_to_all x1, starting transfers between devices, per_device(): lax.all_to_all(outgoing, 'kv', split_axis=0, concat_axis=0, tiled=True)  6 us
    dot_general x4, matrix products, attend(): jnp.einsum('phqsk,pskd->pqhd', softmax_w, value_part, preferred_element_t...  4.94 us
    dynamic_slice x8, local copies, waits for them, and re-layouts, per_device(): lax.map(attend, (queries.reshape(pair_count, 2, BLK, head_count, HD), sel...  4.53 us
    all_to_all x1, starting transfers between devices, swapped_in(): pieces = lax.all_to_all(pieces, mesh_axis, split_axis=0, concat_axis=0)  3.51 us
    dot_general x1, matrix products, per_device(): jnp.dot(swapped_in(scaled, 'tp', 1), w_out, preferred_element_type=jnp.fl...  2.76 us
  transfers between devices with their start and end apart: 3, of which 1 were waited for; matrix products, arithmetic and copies ran while one was open for 13% of the time, Pallas kernels for 0%

profile of v1, /device:TPU:0, one launch (start us, length us, event | category | flops | bytes accessed | tf_op | source)
XLA Modules:
  0.0 78.6 jit_solution(3233516566520393415)
XLA Ops:
  0.0 0.8 %fusion.20 = (s32[8,8]{1,0:T(8,128)S(1)}, s32[8,8]{1,0:T(8,128)S(1)}) fusion(s32[1,8,8]{2,1,0:T(8,128)} %param.15, s32[]{:T(128)S(6)} %axis_index.23), kind=kLoop, calls=%fused_computation.64 | loop fusion | flops 1408 | bytes 772 | tf_op jit(solution)/shard_map/jit(_where)/select_n | solution.py:64
  0.9 0.7 compare_and_fusion.1
  1.7 0.7 copy.39
  2.3 7.3 %all-to-all-start = ((s32[8,1,1]{2,1,0:T(1,128)}), s32[8,1,1]{2,1,0:T(1,128)S(1)}, u32[]{:S(2)}, u32[]{:S(2)}) async-start(s32[8,1,1]{2,1,0:T(1,128)} %copy.39), calls=%async_computation | async-start | bytes 8192 | tf_op jit(solution)/shard_map/all_to_all | solution.py:70
  9.7 0.7 compare_select_fusion
  10.4 1.7 %convolution_bitcast_fusion.1 = f32[512,1,64]{0,2,1:T(8,128)S(1)} fusion(bf16[512,2048]{1,0:T(8,128)(2,1)S(1)} %copy-done, bf16[2048,64]{0,1:T(8,128)(2,1)} %param.11), kind=kOutput, calls=%fused_computation.26 | convolution fusion | flops 134217728 | bytes 2490368 | tf_op jit(solution)/shard_map/dot_general | solution.py:54
  13.0 0.8 convolution_convert_fusion
  13.9 2.0 %fusion.34 = f32[512,256]{0,1:T(8,128)S(1)} fusion(bf16[512,2048]{1,0:T(8,128)(2,1)S(1)} %copy-done, bf16[2048,256]{1,0:T(8,128)(2,1)} %param.10), kind=kOutput, calls=%fused_computation.93 | convolution fusion | flops 536870912 | bytes 3670016 | tf_op jit(solution)/shard_map/dot_general | solution.py:47
  16.4 1.6 %pad_maximum_fusion = bf16[4,2,64,4,64]{2,1,0,4,3:T(2,128)(2,1)} fusion(bf16[4,2,64,4,32]{2,1,0,4,3:T(2,128)(2,1)S(1)} %concatenate.35, bf16[4,2,64,4,32]{2,1,0,4,3:T(2,128)(2,1)S(1)} %concatenate.34), kind=kLoop, calls=%fused_computation.29 | loop fusion | flops 131072 | bytes 524288 | tf_op jit(solution)/shard_map/concatenate | solution.py:29
  19.3 0.7 broadcast_select_fusion
  20.0 6.0 %all-to-all-start.1 = ((bf16[8,64,128]{2,1,0:T(8,128)(2,1)}), bf16[8,64,128]{2,1,0:T(8,128)(2,1)S(1)}, u32[]{:S(2)}, u32[]{:S(2)}) async-start(bf16[8,64,128]{2,1,0:T(8,128)(2,1)} %broadcast_select_fusion), calls=%async_computation.1 | async-start | bytes 262144 | tf_op jit(solution)/shard_map/all_to_all | solution.py:78
  26.1 0.8 dynamic_slice.23
  26.8 6.5 %all-to-all-done.1 = bf16[8,64,128]{2,1,0:T(8,128)(2,1)S(1)} async-done(((bf16[8,64,128]{2,1,0:T(8,128)(2,1)}), bf16[8,64,128]{2,1,0:T(8,128)(2,1)S(1)}, u32[]{:S(2)}, u32[]{:S(2)}) %all-to-all-start.1) | async-done | bytes 131104 | tf_op jit(solution)/shard_map/all_to_all | solution.py:78
  33.5 0.7 gather_fusion.1
  34.3 17.1 %while.11 = (s32[]{:T(128)}, bf16[4,2,64,4,64]{2,4,3,1,0:T(8,128)(2,1)}, bf16[4,2,8,64,128]{4,3,2,1,0:T(8,128)(2,1)S(1)}, pred[4,2,8]{2,1,0:T(4,128)(4,1)S(1)}, ...) while((s32[]{:T(128)}, ...), condition=%wide.region_4.5_spmd.clone, body=%wide.region_1.4_spmd.clone.sunk | while | flops 69369872 | bytes 13193617 | solution.py:107
  35.3 1.0 %constant_dynamic-slice_fusion.4 = bf16[1,2,64,4,64]{2,1,0,4,3:T(2,128)(2,1)S(1)} fusion(bf16[4,2,64,4,64]{2,1,0,4,3:T(2,128)(2,1)} %get-tuple-element.185, s32[]{:T(128)} %get-tuple-element.171), kind=kLoop, calls=%fused_computation.18.clone.1 | loop fusion | bytes 131076 | tf_op jit(solution)/shard_map/while/body/jit(dynamic_index_in_dim)/dynamic_slice | solution.py:107
  37.3 1.2 %fusion.52 = bf16[4,2,64,4,64]{2,4,3,1,0:T(8,128)(2,1)} fusion(bf16[4,2,64,4,64]{2,4,3,1,0:T(8,128)(2,1)} %get-tuple-element.172, s32[]{:T(128)} %get-tuple-element.171, f32[2,4,64,8,64]{2,4,1,3,0:T(8,128)S(1)} %get-tuple-element.161, f32[2,4,64]{2,1,0:T(4,128)S(1)} %fusion.51, f32[2,4,64]{2,1,0:T(4,128)S(1)} %get-tuple-element.162, ...), kind=kOutput, calls=%fused_computation.10.clone.1 | convolution fusion | flops 34373632 | bytes 1446400 | tf_op jit(solution)/shard_map/while/body/eval_jaxpr/phqsk,pskd->pqhd/dot_general | solution.py:102
  39.6 1.0 %constant_dynamic-slice_fusion.4 = bf16[1,2,64,4,64]{2,1,0,4,3:T(2,128)(2,1)S(1)} fusion(bf16[4,2,64,4,64]{2,1,0,4,3:T(2,128)(2,1)} %get-tuple-element.185, s32[]{:T(128)} %get-tuple-element.171), kind=kLoop, calls=%fused_computation.18.clone.1 | loop fusion | bytes 131076 | tf_op jit(solution)/shard_map/while/body/jit(dynamic_index_in_dim)/dynamic_slice | solution.py:107
  41.6 1.2 %fusion.52 = bf16[4,2,64,4,64]{2,4,3,1,0:T(8,128)(2,1)} fusion(bf16[4,2,64,4,64]{2,4,3,1,0:T(8,128)(2,1)} %get-tuple-element.172, s32[]{:T(128)} %get-tuple-element.171, f32[2,4,64,8,64]{2,4,1,3,0:T(8,128)S(1)} %get-tuple-element.161, f32[2,4,64]{2,1,0:T(4,128)S(1)} %fusion.51, f32[2,4,64]{2,1,0:T(4,128)S(1)} %get-tuple-element.162, ...), kind=kOutput, calls=%fused_computation.10.clone.1 | convolution fusion | flops 34373632 | bytes 1446400 | tf_op jit(solution)/shard_map/while/body/eval_jaxpr/phqsk,pskd->pqhd/dot_general | solution.py:102
  43.2 0.6 copy-done.1
  43.8 1.0 %constant_dynamic-slice_fusion.4 = bf16[1,2,64,4,64]{2,1,0,4,3:T(2,128)(2,1)S(1)} fusion(bf16[4,2,64,4,64]{2,1,0,4,3:T(2,128)(2,1)} %get-tuple-element.185, s32[]{:T(128)} %get-tuple-element.171), kind=kLoop, calls=%fused_computation.18.clone.1 | loop fusion | bytes 131076 | tf_op jit(solution)/shard_map/while/body/jit(dynamic_index_in_dim)/dynamic_slice | solution.py:107
  45.9 1.2 %fusion.52 = bf16[4,2,64,4,64]{2,4,3,1,0:T(8,128)(2,1)} fusion(bf16[4,2,64,4,64]{2,4,3,1,0:T(8,128)(2,1)} %get-tuple-element.172, s32[]{:T(128)} %get-tuple-element.171, f32[2,4,64,8,64]{2,4,1,3,0:T(8,128)S(1)} %get-tuple-element.161, f32[2,4,64]{2,1,0:T(4,128)S(1)} %fusion.51, f32[2,4,64]{2,1,0:T(4,128)S(1)} %get-tuple-element.162, ...), kind=kOutput, calls=%fused_computation.10.clone.1 | convolution fusion | flops 34373632 | bytes 1446400 | tf_op jit(solution)/shard_map/while/body/eval_jaxpr/phqsk,pskd->pqhd/dot_general | solution.py:102
  48.1 1.0 %constant_dynamic-slice_fusion.4 = bf16[1,2,64,4,64]{2,1,0,4,3:T(2,128)(2,1)S(1)} fusion(bf16[4,2,64,4,64]{2,1,0,4,3:T(2,128)(2,1)} %get-tuple-element.185, s32[]{:T(128)} %get-tuple-element.171), kind=kLoop, calls=%fused_computation.18.clone.1 | loop fusion | bytes 131076 | tf_op jit(solution)/shard_map/while/body/jit(dynamic_index_in_dim)/dynamic_slice | solution.py:107
  50.2 1.2 %fusion.52 = bf16[4,2,64,4,64]{2,4,3,1,0:T(8,128)(2,1)} fusion(bf16[4,2,64,4,64]{2,4,3,1,0:T(8,128)(2,1)} %get-tuple-element.172, s32[]{:T(128)} %get-tuple-element.171, f32[2,4,64,8,64]{2,4,1,3,0:T(8,128)S(1)} %get-tuple-element.161, f32[2,4,64]{2,1,0:T(4,128)S(1)} %fusion.51, f32[2,4,64]{2,1,0:T(4,128)S(1)} %get-tuple-element.162, ...), kind=kOutput, calls=%fused_computation.10.clone.1 | convolution fusion | flops 34373632 | bytes 1446400 | tf_op jit(solution)/shard_map/while/body/eval_jaxpr/phqsk,pskd->pqhd/dot_general | solution.py:102
  51.4 1.3 %copy.44 = f32[4,2,64,4,64]{4,3,2,1,0:T(4,128)S(1)} copy(bf16[4,2,64,4,64]{2,4,3,1,0:T(8,128)(2,1)} %get-tuple-element.47) | data formatting | bytes 786432 | tf_op jit(solution)/shard_map/convert_element_type | solution.py:117
  52.7 1.4 %reshape.370 = f32[512,256]{1,0:T(8,128)} reshape(f32[4,2,64,4,64]{4,3,2,1,0:T(4,128)S(1)} %copy.44) | data formatting | bytes 1048576 | tf_op jit(solution)/shard_map/convert_element_type | solution.py:117
  54.1 1.1 %multiply_convert_fusion = bf16[512,256]{1,0:T(8,128)(2,1)S(1)} fusion(f32[512,256]{1,0:T(8,128)} %reshape.370, f32[256]{0:T(256)S(1)} %dynamic_slice.23), kind=kLoop, calls=%fused_computation.30 | loop fusion | flops 262144 | bytes 787456 | tf_op jit(solution)/shard_map/convert_element_type | solution.py:120
  55.4 1.1 %stack.2 = bf16[4,512,256]{1,2,0:T(8,128)(2,1)} broadcast(bf16[512,256]{0,1:T(8,128)(2,1)S(1)} %copy.45), dimensions={1,2} | broadcast | bytes 1310720 | tf_op jit(solution)/shard_map/stack | solution.py:16
  56.4 3.5 %all-to-all-start.2 = ((bf16[4,512,256]{1,2,0:T(8,128)(2,1)}), bf16[4,512,256]{1,2,0:T(8,128)(2,1)S(1)}, u32[]{:S(2)}, u32[]{:S(2)}) async-start(bf16[4,512,256]{1,2,0:T(8,128)(2,1)} %stack.2), calls=%async_computation.2 | async-start | bytes 2097152 | tf_op jit(solution)/shard_map/all_to_all | solution.py:17
  60.0 1.2 %multiply_reduce_fusion = f32[4,2,64]{2,1,0:T(2,128)S(1)} fusion(bf16[4,2,64,4,64]{2,4,3,1,0:T(8,128)(2,1)} %get-tuple-element.47), kind=kLoop, calls=%fused_computation.28 | loop fusion | flops 392704 | bytes 264192 | tf_op jit(solution)/shard_map/reduce_sum | solution.py:118
  61.3 14.6 %psum.7 = f32[512]{0:T(512)S(1)} all-reduce(f32[512]{0:T(512)S(1)} %reduce_sum.21), channel_id=1, replica_groups=mesh['kv'=8,'tp'=4] {'tp'}, use_global_device_ids=true, to_apply=%region_6.7 | all-reduce | flops 512 | bytes 4096 | tf_op jit(solution)/shard_map/psum | solution.py:118
  75.8 2.8 %fusion.10 = bf16[512,512]{1,0:T(8,128)(2,1)} fusion(bf16[512,1024]{0,1:T(8,128)(2,1)S(1)} %bitcast.158, bf16[1024,512]{1,0:T(8,128)(2,1)} %param.13, f32[512]{0:T(512)S(1)} %add_rsqrt_fusion), kind=kOutput, calls=%fused_computation.25 | convolution fusion | flops 537395200 | bytes 2623488 | tf_op jit(solution)/shard_map/dot_general | solution.py:121
  (84 shorter events, 10.6 us)
Async XLA Ops:
  0.0 10.4 %copy-start = (bf16[512,2048]{1,0:T(8,128)(2,1)S(1)}, bf16[512,2048]{1,0:T(8,128)(2,1)}, u32[]{:S(2)}) copy-start(bf16[512,2048]{1,0:T(8,128)(2,1)} %param.9) | copy-start | bytes 6291460
  0.0 13.0 %copy-start.3 = (bf16[2048,64]{0,1:T(8,128)(2,1)S(1)}, bf16[2048,64]{0,1:T(8,128)(2,1)}, u32[]{:S(2)}) copy-start(bf16[2048,64]{0,1:T(8,128)(2,1)} %param.12) | copy-start | bytes 786436
  2.3 15.9 %all-to-all-start = ((s32[8,1,1]{2,1,0:T(1,128)}), s32[8,1,1]{2,1,0:T(1,128)S(1)}, u32[]{:S(2)}, u32[]{:S(2)}) async-start(s32[8,1,1]{2,1,0:T(1,128)} %copy.39), calls=%async_computation | async-start | bytes 8192 | tf_op jit(solution)/shard_map/all_to_all | solution.py:70
  15.9 10.9 %copy-start.4 = (s32[1,8,8]{2,1,0:T(8,128)S(1)}, s32[1,8,8]{2,1,0:T(8,128)}, u32[]{:S(2)}) copy-start(s32[1,8,8]{2,1,0:T(8,128)} %param.15) | copy-start | bytes 772
  20.0 13.3 %all-to-all-start.1 = ((bf16[8,64,128]{2,1,0:T(8,128)(2,1)}), bf16[8,64,128]{2,1,0:T(8,128)(2,1)S(1)}, u32[]{:S(2)}, u32[]{:S(2)}) async-start(bf16[8,64,128]{2,1,0:T(8,128)(2,1)} %broadcast_select_fusion), calls=%async_computation.1 | async-start | bytes 262144 | tf_op jit(solution)/shard_map/all_to_all | solution.py:78
  34.3 1.0 %copy-start.1 = (bf16[4,2,8,64,128]{4,3,2,1,0:T(8,128)(2,1)}, bf16[4,2,8,64,128]{4,3,2,1,0:T(8,128)(2,1)S(1)}, u32[]{:S(2)}) copy-start(bf16[4,2,8,64,128]{4,3,2,1,0:T(8,128)(2,1)S(1)} %get-tuple-element.181) | copy-start | bytes 3145732 | tf_op jit(solution)/shard_map/while
  37.3 1.2 %copy-start.2 = (bf16[4,2,8,64,128]{4,3,2,1,0:T(8,128)(2,1)S(1)}, bf16[4,2,8,64,128]{4,3,2,1,0:T(8,128)(2,1)}, u32[]{:S(2)}) copy-start(bf16[4,2,8,64,128]{4,3,2,1,0:T(8,128)(2,1)} %copy-done.1) | copy-start | bytes 3145732 | tf_op jit(solution)/shard_map/while
  38.6 1.0 %copy-start.1 = (bf16[4,2,8,64,128]{4,3,2,1,0:T(8,128)(2,1)}, bf16[4,2,8,64,128]{4,3,2,1,0:T(8,128)(2,1)S(1)}, u32[]{:S(2)}) copy-start(bf16[4,2,8,64,128]{4,3,2,1,0:T(8,128)(2,1)S(1)} %get-tuple-element.181) | copy-start | bytes 3145732 | tf_op jit(solution)/shard_map/while
  41.6 1.2 %copy-start.2 = (bf16[4,2,8,64,128]{4,3,2,1,0:T(8,128)(2,1)S(1)}, bf16[4,2,8,64,128]{4,3,2,1,0:T(8,128)(2,1)}, u32[]{:S(2)}) copy-start(bf16[4,2,8,64,128]{4,3,2,1,0:T(8,128)(2,1)} %copy-done.1) | copy-start | bytes 3145732 | tf_op jit(solution)/shard_map/while
  42.9 1.0 %copy-start.1 = (bf16[4,2,8,64,128]{4,3,2,1,0:T(8,128)(2,1)}, bf16[4,2,8,64,128]{4,3,2,1,0:T(8,128)(2,1)S(1)}, u32[]{:S(2)}) copy-start(bf16[4,2,8,64,128]{4,3,2,1,0:T(8,128)(2,1)S(1)} %get-tuple-element.181) | copy-start | bytes 3145732 | tf_op jit(solution)/shard_map/while
  45.9 1.2 %copy-start.2 = (bf16[4,2,8,64,128]{4,3,2,1,0:T(8,128)(2,1)S(1)}, bf16[4,2,8,64,128]{4,3,2,1,0:T(8,128)(2,1)}, u32[]{:S(2)}) copy-start(bf16[4,2,8,64,128]{4,3,2,1,0:T(8,128)(2,1)} %copy-done.1) | copy-start | bytes 3145732 | tf_op jit(solution)/shard_map/while
  47.1 1.0 %copy-start.1 = (bf16[4,2,8,64,128]{4,3,2,1,0:T(8,128)(2,1)}, bf16[4,2,8,64,128]{4,3,2,1,0:T(8,128)(2,1)S(1)}, u32[]{:S(2)}) copy-start(bf16[4,2,8,64,128]{4,3,2,1,0:T(8,128)(2,1)S(1)} %get-tuple-element.181) | copy-start | bytes 3145732 | tf_op jit(solution)/shard_map/while
  50.2 1.2 %copy-start.2 = (bf16[4,2,8,64,128]{4,3,2,1,0:T(8,128)(2,1)S(1)}, bf16[4,2,8,64,128]{4,3,2,1,0:T(8,128)(2,1)}, u32[]{:S(2)}) copy-start(bf16[4,2,8,64,128]{4,3,2,1,0:T(8,128)(2,1)} %copy-done.1) | copy-start | bytes 3145732 | tf_op jit(solution)/shard_map/while
  56.4 19.4 %all-to-all-start.2 = ((bf16[4,512,256]{1,2,0:T(8,128)(2,1)}), bf16[4,512,256]{1,2,0:T(8,128)(2,1)S(1)}, u32[]{:S(2)}, u32[]{:S(2)}) async-start(bf16[4,512,256]{1,2,0:T(8,128)(2,1)} %stack.2), calls=%async_computation.2 | async-start | bytes 2097152 | tf_op jit(solution)/shard_map/all_to_all | solution.py:17
